TPU v7x, 128 devices: a whole 4x4x4 slice. The times are simulated.
128 devices in a mesh: ep: 128 (over z, y, x, core).
Axes of the slice: x: 4, y: 4, z: 4, core: 2. Of those that a mesh axis runs over, the one named last changes fastest.
Arguments:
- hidden: bfloat16 [4096, 2048], P('ep'), may hold values from -6 to 6
- cache_keys: bfloat16 [4096, 1024, 128], P('ep'), may hold values from -512 to 512
- cache_values: bfloat16 [4096, 1024, 128], P('ep'), may hold values from -6 to 6
- lengths: int32 [4096], P('ep'), may hold values from 1 to 1024
- first_gain: float32 [2048], replicated, may hold values from 0.1 to 1.9
- query_weight: bfloat16 [2048, 1024], replicated, may hold values from -0.125 to 0.125
- key_weight: bfloat16 [2048, 128], replicated, may hold values from -0.125 to 0.125
- value_weight: bfloat16 [2048, 128], replicated, may hold values from -0.125 to 0.125
- mixing: float32 [8], replicated, may hold values from 0.3 to 0.8
- head_gain: float32 [128], replicated, may hold values from 0.1 to 1.9
- out_weight: bfloat16 [1024, 2048], replicated, may hold values from -0.1875 to 0.1875
- second_gain: float32 [2048], replicated, may hold values from 0.1 to 1.9
- routes: int32 [4096, 4], P('ep'), may hold values from 0 to 63, as said below
- route_weight: float32 [4096, 4], P('ep'), may hold values from 0.05 to 1
- expert_gate: bfloat16 [128, 2048, 256], P('ep'), may hold values from -0.125 to 0.125
- expert_up: bfloat16 [128, 2048, 256], P('ep'), may hold values from -0.125 to 0.125
- expert_down: bfloat16 [128, 256, 2048], P('ep'), may hold values from -0.25 to 0.25
Outputs:
- layer_out: bfloat16 [4096, 2048], P('ep')
- new_key: bfloat16 [4096, 128], P('ep')
- new_value: bfloat16 [4096, 128], P('ep')
Inputs may be any that keep to these rules, and one draw needn't show every extreme that they name: `routes`: each row names 4 different experts of one group, that is of one block of 16 consecutive numbers. Among the rows of one device, two rows name the same set of experts or disjoint sets, and no expert is named by more than 4 rows; one and the same expert is named by exactly 4 rows on every device.
All inputs are finite; a program needn't handle non-finite values.
Results may differ from a plain program's by a relative error of at most 0.025.
Values may be sent and summed in bfloat16 or wider, within the bound.
A program may use at most 128 MiB of HBM per device.

v0:
```python
import jax
import jax.numpy as jnp
from jax import lax
from jax.sharding import PartitionSpec as P

D = 2048
HEADS = 8
DK = 64
DV = 128
EXP_SPLIT = 2
TOP_K = 4


epsilon = 1e-06


def root_scale(rows, gain):
    values = rows.astype(jnp.float32)
    factor = lax.rsqrt(jnp.mean(values * values, axis=-1, keepdims=True) + epsilon)
    return values * factor * gain


def slot_tables(routes, experts, capacity):
    count, picks = routes.shape
    flat = routes.reshape(count * picks)
    indicator = (flat[:, None] == jnp.arange(experts, dtype=jnp.int32)[None, :]).astype(jnp.int32)
    before = jnp.cumsum(indicator, axis=0) - indicator
    place = jnp.sum(before * indicator, axis=1)
    target = flat * capacity + place
    slots = jnp.arange(experts * capacity, dtype=jnp.int32)
    match = target[None, :] == slots[:, None]
    return match.reshape(experts * capacity, count, picks)


def attend(query, new_key, new_value, cache_keys, cache_values, lengths, mixing):
    count = query.shape[0]
    span = cache_keys.shape[1]
    queries = query.reshape(count, HEADS, 2, DK)
    keys = cache_keys.reshape(count, span, 2, DK)
    scores = jnp.einsum(
        "shmd,slmd->shml", queries, keys, preferred_element_type=jnp.float32
    ) * DK ** (-0.5)
    own_scores = jnp.einsum(
        "shmd,smd->shm", queries, new_key.reshape(count, 2, DK), preferred_element_type=jnp.float32
    ) * DK ** (-0.5)
    valid = jnp.arange(span, dtype=jnp.int32)[None, :] < lengths[:, None]
    scores = jnp.where(valid[:, None, None, :], scores, -jnp.inf)
    highest = jnp.maximum(jnp.max(scores, axis=-1), own_scores)
    weights = jnp.exp(scores - highest[..., None])
    own_weights = jnp.exp(own_scores - highest)
    total = jnp.sum(weights, axis=-1) + own_weights
    weights = weights / total[..., None]
    own_weights = own_weights / total
    contrast = (weights[:, :, 0] - mixing[None, :, None] * weights[:, :, 1]).astype(jnp.bfloat16)
    own_contrast = (own_weights[:, :, 0] - mixing[None, :] * own_weights[:, :, 1]).astype(
        jnp.bfloat16
    )
    mixed = jnp.einsum("shl,sle->she", contrast, cache_values, preferred_element_type=jnp.float32)
    return (
        mixed
        + own_contrast.astype(jnp.float32)[..., None] * new_value.astype(jnp.float32)[:, None, :]
    )


def head_norm(mixed, head_gain):
    factor = lax.rsqrt(jnp.mean(mixed * mixed, axis=-1, keepdims=True) + epsilon)
    scaled = mixed * factor * head_gain
    return scaled.reshape(mixed.shape[0], HEADS * DV).astype(jnp.bfloat16)


def expert_apply(flat, expert_gate, expert_up, expert_down):
    gate = jnp.dot(flat, expert_gate[0], preferred_element_type=jnp.float32)
    upper = jnp.dot(flat, expert_up[0], preferred_element_type=jnp.float32)
    inner = (jax.nn.silu(gate) * upper).astype(jnp.bfloat16)
    return jnp.dot(inner, expert_down[0], preferred_element_type=jnp.float32).astype(jnp.bfloat16)


def per_device(
    hidden,
    cache_keys,
    cache_values,
    lengths,
    first_gain,
    query_weight,
    key_weight,
    value_weight,
    mixing,
    head_gain,
    out_weight,
    second_gain,
    routes,
    route_weight,
    expert_gate,
    expert_up,
    expert_down,
):
    count = hidden.shape[0]
    normed = root_scale(hidden, first_gain).astype(jnp.bfloat16)
    query = jnp.dot(normed, query_weight, preferred_element_type=jnp.float32).astype(jnp.bfloat16)
    new_key = jnp.dot(normed, key_weight, preferred_element_type=jnp.float32).astype(jnp.bfloat16)
    new_value = jnp.dot(normed, value_weight, preferred_element_type=jnp.float32).astype(
        jnp.bfloat16
    )
    mixed = attend(query, new_key, new_value, cache_keys, cache_values, lengths, mixing)
    head_rows = head_norm(mixed, head_gain)
    update = jnp.dot(head_rows, out_weight, preferred_element_type=jnp.float32)
    residual = (hidden.astype(jnp.float32) + update).astype(jnp.bfloat16)
    expert_input = root_scale(residual, second_gain).astype(jnp.bfloat16)
    experts = lax.axis_size("ep") // EXP_SPLIT
    capacity = max(2, 2 * count * TOP_K // experts)
    match = slot_tables(routes, experts, capacity)
    pick = jnp.sum(match.astype(jnp.int32), axis=2).astype(jnp.bfloat16)
    packed = jnp.dot(pick, expert_input, preferred_element_type=jnp.float32).astype(jnp.bfloat16)
    outgoing = jnp.repeat(packed.reshape(experts, capacity, D), EXP_SPLIT, axis=0)
    rows = lax.all_to_all(outgoing, "ep", split_axis=0, concat_axis=0, tiled=True)
    flat = rows.reshape(-1, rows.shape[2])
    result = expert_apply(flat, expert_gate, expert_up, expert_down)
    returned = lax.all_to_all(
        result.reshape(rows.shape), "ep", split_axis=0, concat_axis=0, tiled=True
    )
    halves = returned.astype(jnp.float32).reshape(experts, EXP_SPLIT, capacity, D)
    expert_out = jnp.sum(halves, axis=1).reshape(experts * capacity, D)
    weighting = jnp.sum(jnp.where(match, route_weight[None, :, :], 0.0), axis=2).T
    routed = jnp.dot(weighting, expert_out, precision=lax.Precision.HIGHEST)
    layer_out = (residual.astype(jnp.float32) + routed).astype(jnp.bfloat16)
    return (layer_out, new_key, new_value)


def solution(mesh):
    return jax.shard_map(
        per_device,
        mesh=mesh,
        in_specs=(
            P("ep", None),
            P("ep", None, None),
            P("ep", None, None),
            P("ep"),
            P(),
            P(),
            P(),
            P(),
            P(),
            P(),
            P(),
            P(),
            P("ep", None),
            P("ep", None),
            P("ep", None, None),
            P("ep", None, None),
            P("ep", None, None),
        ),
        out_specs=(P("ep", None), P("ep", None), P("ep", None)),
        check_vma=False,
    )
```

profile of v0, /device:TPU:0, one launch (start us, length us, event | category | flops | bytes accessed | tf_op | source)
XLA Modules:
  0.0 132.3 jit_solution(4276068016359851897)
XLA Ops:
  0.6 1.1 fusion.22
  1.8 3.2 %convolution_convert_fusion.2 = bf16[32,1024]{1,0:T(8,128)(2,1)S(1)} fusion(bf16[2048,1024]{1,0:T(8,128)(2,1)} %param.22, bf16[32,2048]{1,0:T(8,128)(2,1)} %param.17, f32[2048]{0:T(1024)} %param.21, f32[32]{0:T(128)S(1)} %add_rsqrt_fusion.2), kind=kOutput, calls=%fused_computation.17 | convolution fusion | flops 134512640 | bytes 4399232 | tf_op jit(solution)/shard_map/dot_general | solution.py:99
  5.3 12.0 %copy.41 = bf16[32,1024,128]{1,2,0:T(8,128)(2,1)} copy(bf16[32,1024,128]{2,1,0:T(8,128)(2,1)} %param.18) | data formatting | bytes 16777216 | tf_op args[1]
  17.3 0.3 convolution_convert_fusion.4
  17.8 4.7 %bitcast_reduce_fusion = (f32[32,8,2]{1,2,0:T(2,128)S(1)}, f32[32,2,8,1024]{3,2,1,0:T(8,128)S(1)}) fusion(pred[32,1024]{1,0:T(8,128)(4,1)S(1)} %iota_compare_fusion.1, bf16[32,1024,2,64]{1,3,2,0:T(8,128)(2,1)} %bitcast.79, bf16[32,8,2,64]{3,2,1,0:T(2,128)(2,1)S(1)} %reshape.112), kind=kOutput, calls=%fused_computation.9 | convolution fusion | flops 68681216 | bytes 10586112 | tf_op jit(solution)/shard_map/shmd,slmd->shml/dot_general | solution.py:40
  22.6 0.7 fusion.5
  23.3 0.6 fusion.4
  24.0 0.4 copy-done.5
  24.3 0.9 fusion.44
  25.3 4.9 %multiply_reduce_fusion.1 = (f32[32,8]{1,0:T(8,128)S(1)}, f32[32,8,128]{2,1,0:T(8,128)S(1)}) fusion(f32[32,128]{1,0:T(8,128)S(1)} %get-tuple-element.7, f32[32,8]{1,0:T(8,128)S(1)} %bitcast.84, bf16[32,1024,128]{2,1,0:T(8,128)(2,1)} %param.19, f32[32,8,2,1024]{3,1,2,0:T(8,128)S(1)} %fusion.4, f32[8]{0:T(128)S(1)} %copy-done.10), kind=kOutput, calls=%fused_computation.49 | convolution fusion | flops 68026112 | bytes 10635296 | tf_op jit(solution)/shard_map/shl,sle->she/dot_general | solution.py:58
  30.3 0.9 multiply_reduce_fusion
  32.3 0.5 convolution_convert_fusion.1
  32.7 0.4 reshape.115
  33.2 1.2 broadcast_in_dim.26
  34.4 41.3 %all_to_all.10 = bf16[128,4,2048]{2,1,0:T(4,128)(2,1)S(1)} all-to-all(bf16[128,4,2048]{2,1,0:T(4,128)(2,1)S(1)} %bitcast.80), channel_id=1, replica_groups=mesh['ep'=128] {'ep'}, dimensions={0} | all-to-all | bytes 4194304 | tf_op jit(solution)/shard_map/all_to_all | solution.py:115
  75.8 2.1 %reshape.117 = bf16[512,2048]{1,0:T(8,128)(2,1)} reshape(bf16[128,4,2048]{2,1,0:T(4,128)(2,1)S(1)} %all_to_all.10) | data formatting | bytes 4194304 | tf_op jit(solution)/shard_map/reshape | solution.py:116
  77.8 3.5 %fusion.13 = f32[512,256]{1,0:T(8,128)} fusion(bf16[512,2048]{1,0:T(8,128)(2,1)} %reshape.117, bf16[1,2048,256]{2,1,0:T(8,128)(2,1)} %param.31), kind=kOutput, calls=%fused_computation.27 | convolution fusion | flops 536870912 | bytes 3670016 | tf_op jit(solution)/shard_map/dot_general | solution.py:72
  81.3 5.0 %convolution_convert_fusion = bf16[512,2048]{1,0:T(8,128)(2,1)} fusion(bf16[512,2048]{1,0:T(8,128)(2,1)S(1)} %copy-done.3, bf16[1,256,2048]{2,1,0:T(8,128)(2,1)S(1)} %copy-done, bf16[1,2048,256]{2,1,0:T(8,128)(2,1)} %param.32, f32[512,256]{1,0:T(8,128)} %fusion.13), kind=kOutput, calls=%fused_computation.1 | convolution fusion | flops 1075576832 | bytes 6815744 | tf_op jit(solution)/shard_map/dot_general | solution.py:75
  86.4 4.1 %reshape.118 = bf16[128,4,2048]{2,1,0:T(4,128)(2,1)} reshape(bf16[512,2048]{1,0:T(8,128)(2,1)} %convolution_convert_fusion) | data formatting | bytes 4194304 | tf_op jit(solution)/shard_map/reshape | solution.py:119
  90.5 5.0 %all-to-all-start.1 = ((bf16[128,4,2048]{2,1,0:T(4,128)(2,1)}), bf16[128,4,2048]{2,1,0:T(4,128)(2,1)S(1)}, u32[]{:S(2)}, u32[]{:S(2)}) async-start(bf16[128,4,2048]{2,1,0:T(4,128)(2,1)} %reshape.118), calls=%async_computation.1 | async-start | bytes 4194304 | tf_op jit(solution)/shard_map/all_to_all | solution.py:118
  95.6 30.1 %all-to-all-done.1 = bf16[128,4,2048]{2,1,0:T(4,128)(2,1)S(1)} async-done(((bf16[128,4,2048]{2,1,0:T(4,128)(2,1)}), bf16[128,4,2048]{2,1,0:T(4,128)(2,1)S(1)}, u32[]{:S(2)}, u32[]{:S(2)}) %all-to-all-start.1) | async-done | bytes 2097184 | tf_op jit(solution)/shard_map/all_to_all | solution.py:118
  125.6 2.7 %convert_reduce_fusion = f32[64,4,2048]{2,1,0:T(4,128)} fusion(bf16[128,4,2048]{2,1,0:T(4,128)(2,1)S(1)} %all-to-all-done.1), kind=kLoop, calls=%fused_computation | loop fusion | flops 1572864 | bytes 4194304 | tf_op jit(solution)/shard_map/reduce_sum | solution.py:122
  128.3 2.0 %reshape.121 = f32[256,2048]{1,0:T(8,128)S(1)} reshape(f32[64,4,2048]{2,1,0:T(4,128)} %convert_reduce_fusion) | data formatting | bytes 4194304 | tf_op jit(solution)/shard_map/reshape | solution.py:122
  130.3 2.0 %fusion.2 = bf16[32,2048]{1,0:T(8,128)(2,1)} fusion(f32[32,2048]{1,0:T(8,128)S(1)} %get-tuple-element.12, f32[256,32]{0,1:T(8,128)S(1)} %select_reduce_fusion, f32[256,2048]{1,0:T(8,128)S(1)} %reshape.121), kind=kOutput, calls=%fused_computation.7 | convolution fusion | flops 201457664 | bytes 2523136 | tf_op jit(solution)/shard_map/dot_general | solution.py:124
  (48 shorter events, 1.8 us)
Async XLA Ops:
  0.6 80.7 %copy-start = (bf16[1,256,2048]{2,1,0:T(8,128)(2,1)S(1)}, bf16[1,256,2048]{2,1,0:T(8,128)(2,1)}, u32[]{:S(2)}) copy-start(bf16[1,256,2048]{2,1,0:T(8,128)(2,1)} %param.33) | copy-start | bytes 3145732
  1.8 3.3 %copy-start.12 = (s32[32]{0:T(128)S(1)}, s32[32]{0:T(128)}, u32[]{:S(2)}) copy-start(s32[32]{0:T(128)} %param.20) | copy-start | bytes 388
  5.2 12.0 %copy-start.2 = (bf16[32,2048]{1,0:T(8,128)(2,1)S(1)}, bf16[32,2048]{1,0:T(8,128)(2,1)}, u32[]{:S(2)}) copy-start(bf16[32,2048]{1,0:T(8,128)(2,1)} %param.17) | copy-start | bytes 393220
  5.2 12.0 %copy-start.4 = (bf16[2048,128]{1,0:T(8,128)(2,1)S(1)}, bf16[2048,128]{1,0:T(8,128)(2,1)}, u32[]{:S(2)}) copy-start(bf16[2048,128]{1,0:T(8,128)(2,1)} %param.23) | copy-start | bytes 1572868
  5.2 12.0 %copy-start.6 = (f32[2048]{0:T(1024)S(1)}, f32[2048]{0:T(1024)}, u32[]{:S(2)}) copy-start(f32[2048]{0:T(1024)} %param.21) | copy-start | bytes 24580
  17.5 5.0 %copy-start.7 = (bf16[32,128]{1,0:T(8,128)(2,1)}, bf16[32,128]{1,0:T(8,128)(2,1)S(1)}, u32[]{:S(2)}) copy-start(bf16[32,128]{1,0:T(8,128)(2,1)S(1)} %convolution_convert_fusion.4) | copy-start | bytes 24580
  23.3 1.0 copy-start.5
  23.3 1.9 %copy-start.10 = (f32[8]{0:T(128)S(1)}, f32[8]{0:T(128)}, u32[]{:S(2)}) copy-start(f32[8]{0:T(128)} %param.25) | copy-start | bytes 100
  25.2 5.0 %copy-start.13 = (f32[128]{0:T(128)S(1)}, f32[128]{0:T(128)}, u32[]{:S(2)}) copy-start(f32[128]{0:T(128)} %param.26) | copy-start | bytes 1540
  25.2 5.1 %copy-start.1 = (bf16[1024,2048]{1,0:T(8,128)(2,1)S(1)}, bf16[1024,2048]{1,0:T(8,128)(2,1)}, u32[]{:S(2)}) copy-start(bf16[1024,2048]{1,0:T(8,128)(2,1)} %param.27) | copy-start | bytes 12582916
  30.3 1.0 copy-start.9
  30.3 1.9 %copy-start.8 = (f32[2048]{0:T(1024)S(1)}, f32[2048]{0:T(1024)}, u32[]{:S(2)}) copy-start(f32[2048]{0:T(1024)} %param.28) | copy-start | bytes 24580
  77.8 3.5 %copy-start.3 = (bf16[512,2048]{1,0:T(8,128)(2,1)S(1)}, bf16[512,2048]{1,0:T(8,128)(2,1)}, u32[]{:S(2)}) copy-start(bf16[512,2048]{1,0:T(8,128)(2,1)} %reshape.117) | copy-start | bytes 6291460
  90.5 5.0 %copy-start.11 = (f32[32,4]{0,1:T(4,128)S(1)}, f32[32,4]{0,1:T(4,128)}, u32[]{:S(2)}) copy-start(f32[32,4]{0,1:T(4,128)} %param.30) | copy-start | bytes 1540
  90.5 35.1 %all-to-all-start.1 = ((bf16[128,4,2048]{2,1,0:T(4,128)(2,1)}), bf16[128,4,2048]{2,1,0:T(4,128)(2,1)S(1)}, u32[]{:S(2)}, u32[]{:S(2)}) async-start(bf16[128,4,2048]{2,1,0:T(4,128)(2,1)} %reshape.118), calls=%async_computation.1 | async-start | bytes 4194304 | tf_op jit(solution)/shard_map/all_to_all | solution.py:118
where the time goes:
time: 133 us; the launch traced here: 132 us
  blocking collectives  41.3 us (31%)
  waiting for transfers between devices  30.1 us (23%)
  matrix products  26 us (20%)
  local copies, waits for them, and re-layouts  22.9 us (17%)
  other arithmetic  6.08 us (5%)
  starting transfers between devices  4.96 us (4%)
    all_to_all x1, blocking collectives, per_device(): lax.all_to_all(outgoing, 'ep', split_axis=0, concat_axis=0, tiled=True)  41.3 us
    all_to_all x1, waiting for transfers between devices, per_device(): lax.all_to_all(result.reshape(rows.shape), 'ep', split_axis=0, concat_axi...  30.1 us
    unnamed x30, local copies, waits for them, and re-layouts  12.6 us
    dot_general x1, matrix products, expert_apply(): jnp.dot(inner, expert_down[0], preferred_element_type=jnp.float32)  5.02 us
    all_to_all x1, starting transfers between devices, per_device(): lax.all_to_all(result.reshape(rows.shape), 'ep', split_axis=0, concat_axi...  4.96 us
    dot_general x1, matrix products, attend(): jnp.einsum('shl,sle->she', contrast, cache_values, preferred_element_type...  4.9 us
    dot_general x1, matrix products, attend(): jnp.einsum('shmd,slmd->shml', queries, keys, preferred_element_type=jnp.f...  4.69 us
    reshape x1, local copies, waits for them, and re-layouts, per_device(): result.reshape(rows.shape)  4.12 us
  transfers between devices with their start and end apart: 1, of which 1 were waited for; matrix products, arithmetic and copies ran while one was open for 0% of the time, Pallas kernels for 0%

commit v1 on v0

v1 whole, which is shorter than its diff:
```python
import functools

import jax
import jax.numpy as jnp
from jax import lax
from jax.experimental import pallas as pl
from jax.experimental.pallas import tpu as pltpu
from jax.sharding import PartitionSpec as P

MESH = pl.DeviceIdType.MESH
BF16 = jnp.bfloat16
F32 = jnp.float32

D = 2048
HEADS = 8
DK = 64
DV = 128
PART = 256
TOP_K = 4
SEQS = 32
SPAN = 1024
CAP = 4
CHIPS = 64
SIDE = 4
GROUP = 8
GROUPS = SEQS // GROUP
WCHUNKS = 4
PIECES = 2
WIDTH = D // PIECES
ROWS = CAP * PIECES
BLOCKS = 4
PER = CHIPS // BLOCKS
MUL = 37
INV = pow(MUL, -1, CHIPS)
LANES = GROUP * HEADS * 2
EPS = 1e-06


def dot(a, b, dims=((1,), (0,))):
    return lax.dot_general(a, b, (dims, ((), ())), preferred_element_type=F32)


def iota(shape, axis):
    return lax.broadcasted_iota(jnp.int32, shape, axis)


def row_scale(values):
    return lax.rsqrt(jnp.mean(values * values, axis=-1, keepdims=True) + EPS)


def kernel(
    hidden_h, keys_h, values_h, lengths_h, gain1_h, wq_h, wk_h, wv_h, mixing_h, hgain_h, wo_h, gain2_h,
    routes_h, rweight_h, gate_h, up_h, down_h,
    out_h, nkey_h, nvalue_h,
    hidden, kbuf, vbuf, lens, gain1, wq, wk, wv, mixing, hgain, wo, gain2, routes, rweight, wg, wu, wd,
    qbuf, nkbuf, nvbuf, scores, contrast, heads, resid, outbuf, nkout, nvout,
    wcomb, sendbuf, recvbuf, ybuf, retbuf,
    small_sem, wq_sem, k_sem, v_sem, wo_sem, exp_sem, out_sem,
    wsend_sem, wrecv_sem, dsend_sem, drecv_sem, rsend_sem, rrecv_sem,
):
    me = lax.axis_index("ep")
    core = lax.rem(me, 2)
    chip = lax.div(me, 2)
    cx = lax.rem(chip, SIDE)
    cy = lax.rem(lax.div(chip, SIDE), SIDE)
    cz = lax.div(chip, SIDE * SIDE)
    sibling = chip * 2 + (1 - core)

    def partner(k, sign):
        rel = lax.rem(k * INV, CHIPS)
        dx = lax.rem(rel, SIDE)
        dy = lax.rem(lax.div(rel, SIDE), SIDE)
        dz = lax.div(rel, SIDE * SIDE)
        x = lax.rem(cx + sign * dx + SIDE, SIDE)
        y = lax.rem(cy + sign * dy + SIDE, SIDE)
        z = lax.rem(cz + sign * dz + SIDE, SIDE)
        return ((z * SIDE + y) * SIDE + x) * 2 + core

    barrier = pltpu.get_barrier_semaphore()

    def greet(k, carry):
        pl.semaphore_signal(barrier, inc=1, device_id=(partner(k, 1),), device_id_type=MESH)
        return carry

    lax.fori_loop(1, CHIPS, greet, 0)
    pl.semaphore_signal(barrier, inc=1, device_id=(sibling,), device_id_type=MESH)

    smalls = [
        (hidden_h, hidden), (gain1_h, gain1), (wk_h, wk), (wv_h, wv), (lengths_h, lens), (mixing_h, mixing),
        (hgain_h, hgain), (gain2_h, gain2), (routes_h, routes), (rweight_h, rweight),
    ]
    small = [pltpu.make_async_copy(a, b, small_sem.at[i]) for i, (a, b) in enumerate(smalls)]
    small[0].start()
    small[1].start()
    step = D // WCHUNKS
    wq_copies = [
        pltpu.make_async_copy(wq_h.at[pl.ds(i * step, step)], wq.at[pl.ds(i * step, step)], wq_sem.at[i])
        for i in range(WCHUNKS)
    ]
    for copy in wq_copies:
        copy.start()
    for copy in small[2:]:
        copy.start()

    def fetch(g, carry):
        for s in range(GROUP):
            pltpu.make_async_copy(keys_h.at[g * GROUP + s], kbuf.at[g, :, pl.ds(s * 2 * DK, 2 * DK)], k_sem.at[g]).start()
        for s in range(GROUP):
            pltpu.make_async_copy(values_h.at[g * GROUP + s], vbuf.at[g, :, pl.ds(s * DV, DV)], v_sem.at[g]).start()
        return carry

    own = [
        pltpu.make_async_copy(gate_h.at[0], wg.at[core], exp_sem.at[0]),
        pltpu.make_async_copy(up_h.at[0], wu.at[core], exp_sem.at[1]),
        pltpu.make_async_copy(down_h.at[0], wd.at[core], exp_sem.at[2]),
    ]
    wo_copy = pltpu.make_async_copy(wo_h, wo, wo_sem)
    fetch(0, 0)
    for copy in own:
        copy.start()
    lax.fori_loop(1, GROUPS, fetch, 0)
    wo_copy.start()

    small[0].wait()
    small[1].wait()
    values = hidden[...].astype(F32)
    normed = (values * row_scale(values) * gain1[...]).astype(BF16)
    query = jnp.zeros((SEQS, HEADS * 2 * DK), F32)
    for i in range(WCHUNKS):
        wq_copies[i].wait()
        query += dot(normed[:, i * step : (i + 1) * step], wq[i * step : (i + 1) * step, :])
    qbuf[...] = query.astype(BF16).astype(F32) * DK ** (-0.5)
    for copy in small[2:]:
        copy.wait()
    new_key = dot(normed, wk[...]).astype(BF16)
    new_value = dot(normed, wv[...]).astype(BF16)
    nkout[...] = new_key
    nvout[...] = new_value
    nkbuf[...] = new_key.astype(F32)
    nvbuf[...] = new_value.astype(F32)
    key_copy = pltpu.make_async_copy(nkout, nkey_h, out_sem.at[0])
    value_copy = pltpu.make_async_copy(nvout, nvalue_h, out_sem.at[1])
    key_copy.start()
    value_copy.start()

    lanes = PIECES * SEQS
    spread = (iota((SEQS, lanes), 0) == lax.rem(iota((SEQS, lanes), 1), SEQS)).astype(BF16)
    picks = dot(routes[...].astype(F32).astype(BF16), spread).astype(jnp.int32)
    lowest = jnp.min(picks, axis=0, keepdims=True)
    named = (iota((CHIPS, lanes), 0) == lowest).astype(F32)
    earlier = (iota((lanes, lanes), 0) < lax.rem(iota((lanes, lanes), 1), SEQS)).astype(F32)
    before = dot(named.astype(BF16), earlier.astype(BF16))
    place = jnp.sum(before * named, axis=0, keepdims=True).astype(jnp.int32)
    ex = lax.rem(picks, SIDE)
    ey = lax.rem(lax.div(picks, SIDE), SIDE)
    ez = lax.div(picks, SIDE * SIDE)
    offset = (
        lax.rem(ez - cz + SIDE, SIDE) * (SIDE * SIDE) + lax.rem(ey - cy + SIDE, SIDE) * SIDE + lax.rem(ex - cx + SIDE, SIDE)
    )
    piece = lax.div(iota((1, lanes), 1), SEQS)
    target = lax.rem(offset * MUL, CHIPS) * ROWS + piece * CAP + place
    high = rweight[...].astype(BF16)
    low = (rweight[...] - high.astype(F32)).astype(BF16)
    high = dot(high, spread)
    low = dot(low, spread)
    slot = iota((CHIPS * ROWS, lanes), 0)
    pick = jnp.zeros((CHIPS * ROWS, lanes), F32)
    comb_high = jnp.zeros((CHIPS * ROWS, lanes), F32)
    comb_low = jnp.zeros((CHIPS * ROWS, lanes), F32)
    for k in range(TOP_K):
        hit = slot == target[k : k + 1, :]
        pick = jnp.where(hit, 1.0, pick)
        comb_high = jnp.where(hit, high[k : k + 1, :], comb_high)
        comb_low = jnp.where(hit, low[k : k + 1, :], comb_low)
    pick = pick.astype(BF16)
    wcomb[...] = jnp.transpose(jnp.concatenate([comb_high, comb_low], axis=1)).astype(BF16)

    pl.semaphore_wait(barrier, CHIPS)

    def share(source, index):
        return pltpu.make_async_remote_copy(
            src_ref=source.at[core], dst_ref=source.at[core], send_sem=wsend_sem.at[index],
            recv_sem=wrecv_sem.at[index], device_id=(sibling,), device_id_type=MESH,
        )

    lane = iota((1, LANES), 1)
    lane_seq = lax.rem(lane, GROUP)
    lane_head = lax.rem(lax.div(lane, GROUP), HEADS)
    mix = jnp.zeros((1, LANES), F32)
    for h in range(HEADS):
        mix = jnp.where(lane_head == h, mixing[h], mix)
    mix = jnp.where(lane < LANES // 2, 1.0, mix)
    row = iota((LANES, 2 * DK), 0)
    col = iota((LANES, 2 * DK), 1)
    same_map = lax.div(row, LANES // 2) == lax.div(col, DK)
    row_seq = lax.rem(row, GROUP)

    def attend(g, carry):
        first = pl.multiple_of(g * GROUP, GROUP)
        rows = [qbuf[pl.ds(first, GROUP), h * 2 * DK : (h + 1) * 2 * DK] for h in range(HEADS)]
        block = jnp.concatenate(rows + rows, axis=0)
        block = jnp.where(same_map, block, 0.0)
        diag = jnp.concatenate(
            [jnp.where(row_seq == s, block, 0.0).astype(BF16) for s in range(GROUP)], axis=1
        )
        limit = jnp.zeros((1, LANES), jnp.int32)
        for s in range(GROUP):
            limit = jnp.where(lane_seq == s, lens[g * GROUP + s], limit)
        fresh = nkbuf[pl.ds(first, GROUP), :]
        fresh_rows = jnp.concatenate(
            [jnp.where(iota((GROUP, 2 * DK), 0) == s, fresh, 0.0).astype(BF16) for s in range(GROUP)], axis=1
        )
        own_score = jnp.sum(dot(fresh_rows, diag, ((1,), (1,))), axis=0, keepdims=True)
        pltpu.make_async_copy(kbuf.at[g], kbuf.at[g], k_sem.at[g]).wait()
        score = dot(kbuf[g], diag, ((1,), (1,)))
        score = jnp.where(iota((SPAN, LANES), 0) < limit, score, -jnp.inf)
        scores[...] = score
        highest = jnp.maximum(jnp.max(score, axis=0, keepdims=True), own_score)
        weight = jnp.exp(scores[...] - highest)
        scores[...] = weight
        own_weight = jnp.exp(own_score - highest)
        total = jnp.sum(weight, axis=0, keepdims=True) + own_weight
        factor = mix / total
        part = scores[...] * factor
        contrast[...] = (part - pltpu.roll(part, LANES // 2, 1)).astype(BF16)
        own_part = own_weight * factor
        own_contrast = own_part - pltpu.roll(own_part, LANES // 2, 1)
        pltpu.make_async_copy(vbuf.at[g], vbuf.at[g], v_sem.at[g]).wait()
        full = dot(contrast[...], vbuf[g], ((0,), (0,)))[: LANES // 2]
        own_rows = jnp.where(iota((GROUP, LANES), 0) == lane_seq, own_contrast, 0.0).astype(BF16)
        mixed = dot(own_rows, nvbuf[pl.ds(first, GROUP), :].astype(BF16), ((0,), (0,)))[: LANES // 2]
        out_seq = lax.rem(iota((LANES // 2, DV), 0), GROUP)
        for s in range(GROUP):
            mixed += jnp.where(out_seq == s, full[:, s * DV : (s + 1) * DV], 0.0)
        normal = mixed * row_scale(mixed) * hgain[...]
        for h in range(HEADS):
            heads[pl.ds(first, GROUP), h * DV : (h + 1) * DV] = normal[h * GROUP : (h + 1) * GROUP]

        @pl.when(g == 0)
        def _():
            for copy in own:
                copy.wait()
            for i, ref in enumerate((wg, wu, wd)):
                share(ref, i).start()

        return carry

    lax.fori_loop(0, GROUPS, attend, 0)

    wo_copy.wait()
    update = dot(heads[...].astype(BF16), wo[...])
    residual = (hidden[...].astype(F32) + update).astype(BF16)
    values = residual.astype(F32)
    resid[...] = values
    given = values * row_scale(values) * gain2[...]
    stacked = jnp.concatenate([given[:, c * WIDTH : (c + 1) * WIDTH] for c in range(PIECES)], axis=0).astype(BF16)
    packed = dot(pick, stacked).astype(BF16).reshape(CHIPS, ROWS, WIDTH)
    sendbuf[...] = packed
    recvbuf[0] = sendbuf[0]

    def dispatch(k, carry):
        pltpu.make_async_remote_copy(
            src_ref=sendbuf.at[k], dst_ref=recvbuf.at[k], send_sem=dsend_sem, recv_sem=drecv_sem.at[lax.div(k, PER)],
            device_id=(partner(k, 1),), device_id_type=MESH,
        ).start()
        return carry

    lax.fori_loop(1, CHIPS, dispatch, 0)

    for i, ref in enumerate((wg, wu, wd)):
        share(ref, i).wait()

    size = PER * ROWS
    line = iota((size, size), 0)
    column = iota((size, size), 1)

    def shuffled(a):
        return lax.rem(lax.div(a, CAP), PIECES) * (PER * CAP) + lax.div(a, ROWS) * CAP + lax.rem(a, CAP)

    to_pieces = (line == shuffled(column)).astype(BF16)
    to_messages = (shuffled(line) == column).astype(BF16)
    tall = PER * CAP

    def expert(b, carry):
        pieces = dot(to_pieces, recvbuf[pl.ds(b * PER, PER)].reshape(size, WIDTH)).astype(BF16)
        inner = []
        for j in range(2):
            gate = jnp.zeros((tall, PART), F32)
            upper = jnp.zeros((tall, PART), F32)
            for c in range(PIECES):
                flat = pieces[c * tall : (c + 1) * tall]
                gate += dot(flat, wg[j, c * WIDTH : (c + 1) * WIDTH, :])
                upper += dot(flat, wu[j, c * WIDTH : (c + 1) * WIDTH, :])
            inner.append((gate / (1.0 + jnp.exp(-gate)) * upper).astype(BF16))
        result = []
        for c in range(PIECES):
            cut = slice(c * WIDTH, (c + 1) * WIDTH)
            result.append((dot(inner[0], wd[0, :, cut]) + dot(inner[1], wd[1, :, cut])).astype(BF16))
        ybuf[pl.ds(b * PER, PER)] = dot(to_messages, jnp.concatenate(result, axis=0)).astype(BF16).reshape(PER, ROWS, WIDTH)

        def give(k, inside):
            pltpu.make_async_remote_copy(
                src_ref=ybuf.at[k], dst_ref=retbuf.at[k], send_sem=rsend_sem, recv_sem=rrecv_sem.at[b],
                device_id=(partner(k, -1),), device_id_type=MESH,
            ).start()
            return inside

        lax.fori_loop(jnp.maximum(b * PER, 1), (b + 1) * PER, give, 0)
        return carry

    def landed(ref, first, count, sem):
        part = ref.at[pl.ds(first, count)]
        pltpu.make_async_copy(part, part, sem).wait()

    landed(recvbuf, 1, PER - 1, drecv_sem.at[0])
    expert(0, 0)
    retbuf[0] = ybuf[0]

    def later(b, carry):
        landed(recvbuf, b * PER, PER, drecv_sem.at[b])
        return expert(b, carry)

    lax.fori_loop(1, BLOCKS, later, 0)

    total = jnp.zeros((2 * lanes, WIDTH), F32)
    for b in range(BLOCKS):
        if b == 0:
            landed(retbuf, 1, PER - 1, rrecv_sem.at[0])
        else:
            landed(retbuf, b * PER, PER, rrecv_sem.at[b])
        total += dot(wcomb[:, b * size : (b + 1) * size], retbuf[b * PER : (b + 1) * PER].reshape(size, WIDTH))
    routed = total[:lanes] + total[lanes:]
    for c in range(PIECES):
        cut = slice(c * WIDTH, (c + 1) * WIDTH)
        outbuf[:, cut] = (resid[:, cut] + routed[c * SEQS : (c + 1) * SEQS]).astype(BF16)
    out_copy = pltpu.make_async_copy(outbuf, out_h, out_sem.at[2])
    out_copy.start()
    landed(sendbuf, 1, CHIPS - 1, dsend_sem)
    landed(ybuf, 1, CHIPS - 1, rsend_sem)
    key_copy.wait()
    value_copy.wait()
    out_copy.wait()


def per_device(
    hidden, cache_keys, cache_values, lengths, first_gain, query_weight, key_weight, value_weight, mixing, head_gain,
    out_weight, second_gain, routes, route_weight, expert_gate, expert_up, expert_down,
):
    args = (
        hidden, cache_keys, cache_values, lengths, first_gain.reshape(1, D), query_weight, key_weight, value_weight,
        mixing, head_gain.reshape(1, DV), out_weight, second_gain.reshape(1, D), routes.T, route_weight.T,
        expert_gate, expert_up, expert_down,
    )
    vmem = pltpu.VMEM
    sem = pltpu.SemaphoreType.DMA
    scratch = [
        vmem((SEQS, D), BF16), vmem((GROUPS, SPAN, GROUP * 2 * DK), BF16), vmem((GROUPS, SPAN, GROUP * DV), BF16),
        pltpu.SMEM((SEQS,), jnp.int32), vmem((1, D), F32), vmem((D, HEADS * 2 * DK), BF16), vmem((D, 2 * DK), BF16),
        vmem((D, DV), BF16), pltpu.SMEM((HEADS,), F32), vmem((1, DV), F32), vmem((HEADS * DV, D), BF16),
        vmem((1, D), F32), vmem((TOP_K, SEQS), jnp.int32), vmem((TOP_K, SEQS), F32),
        vmem((2, D, PART), BF16), vmem((2, D, PART), BF16), vmem((2, PART, D), BF16),
        vmem((SEQS, HEADS * 2 * DK), F32), vmem((SEQS, 2 * DK), F32), vmem((SEQS, DV), F32),
        vmem((SPAN, LANES), F32), vmem((SPAN, LANES), BF16), vmem((SEQS, HEADS * DV), F32), vmem((SEQS, D), F32),
        vmem((SEQS, D), BF16), vmem((SEQS, 2 * DK), BF16), vmem((SEQS, DV), BF16),
        vmem((2 * PIECES * SEQS, CHIPS * ROWS), BF16),
        vmem((CHIPS, ROWS, WIDTH), BF16), vmem((CHIPS, ROWS, WIDTH), BF16),
        vmem((CHIPS, ROWS, WIDTH), BF16), vmem((CHIPS, ROWS, WIDTH), BF16),
        sem((10,)), sem((WCHUNKS,)), sem((GROUPS,)), sem((GROUPS,)), sem, sem((3,)), sem((3,)),
        sem((3,)), sem((3,)), sem, sem((BLOCKS,)), sem, sem((BLOCKS,)),
    ]
    return pl.pallas_call(
        kernel,
        out_shape=(
            jax.ShapeDtypeStruct((SEQS, D), BF16),
            jax.ShapeDtypeStruct((SEQS, 2 * DK), BF16),
            jax.ShapeDtypeStruct((SEQS, DV), BF16),
        ),
        in_specs=[pl.BlockSpec(memory_space=pl.ANY)] * len(args),
        out_specs=[pl.BlockSpec(memory_space=pl.ANY)] * 3,
        scratch_shapes=scratch,
        compiler_params=pltpu.CompilerParams(
            collective_id=0, has_side_effects=True, vmem_limit_bytes=60 * 1024 * 1024
        ),
        name="layer",
    )(*args)


def solution(mesh):
    return jax.shard_map(
        per_device,
        mesh=mesh,
        in_specs=(
            P("ep", None), P("ep", None, None), P("ep", None, None), P("ep"), P(), P(), P(), P(), P(), P(), P(), P(),
            P("ep", None), P("ep", None), P("ep", None, None), P("ep", None, None), P("ep", None, None),
        ),
        out_specs=(P("ep", None), P("ep", None), P("ep", None)),
        check_vma=False,
    )
```

time: 133 us -> 55.9 us (0.42)
  Pallas kernels: 0 us -> 50.8 us
  blocking collectives: 41.3 us -> 0 us
  waiting for transfers between devices: 30.1 us -> 0 us
  matrix products: 26 us -> 0 us
  local copies, waits for them, and re-layouts: 22.9 us -> 4.16 us
  other arithmetic: 6.08 us -> 0 us
  starting transfers between devices: 4.96 us -> 0 us
    pallas_call x0 -> x1, Pallas kernels: none -> 50.8 us  [per_device(): pl.pallas_call(kernel, out_shape=(jax.ShapeDtypeStruct((SEQS, D), BF16),...]
    all_to_all x1 -> x0, blocking collectives: 41.3 us -> none  [per_device(): lax.all_to_all(outgoing, 'ep', split_axis=0, concat_axis=0, tiled=True)]
    all_to_all x1 -> x0, waiting for transfers between devices: 30.1 us -> none  [per_device(): lax.all_to_all(result.reshape(rows.shape), 'ep', split_axis=0, concat_axi...]
    dot_general x11 -> x0, matrix products: 26 us -> none  [the longest x1 5.02 us: expert_apply(): jnp.dot(inner, expert_down[0], preferred_element_type=jnp.float32)]
    reshape x6 -> x0, local copies, waits for them, and re-layouts: 8.81 us -> none  [the longest x1 4.12 us: per_device(): result.reshape(rows.shape)]
    unnamed x30 -> x3, local copies, waits for them, and re-layouts: 12.6 us -> 4.16 us
    all_to_all x1 -> x0, starting transfers between devices: 4.96 us -> none  [per_device(): lax.all_to_all(result.reshape(rows.shape), 'ep', split_axis=0, concat_axi...]
    reduce_sum x6 -> x0, other arithmetic: 4.86 us -> none  [the longest x1 2.69 us: per_device(): expert_out = jnp.sum(halves, axis=1).reshape(experts * capacity, D)]
  transfers between devices with their start and end apart: 1 -> 0, of which waited for: 1 -> 0; matrix products, arithmetic and copies ran while one was open for 0% -> 0% of each run, Pallas kernels for 0% -> 0%
where the time goes in v1:
time: 55.9 us; the launch traced here: 55.6 us
  Pallas kernels  50.8 us (91%)
  local copies, waits for them, and re-layouts  4.16 us (7%)
  between operations  0.65 us (1%)
    pallas_call x1, Pallas kernels, per_device(): pl.pallas_call(kernel, out_shape=(jax.ShapeDtypeStruct((SEQS, D), BF16),...  50.8 us
    unnamed x3, local copies, waits for them, and re-layouts  4.16 us

profile of v1, /device:TPU:0, one launch (start us, length us, event | category | flops | bytes accessed | tf_op | source)
XLA Modules:
  0.0 55.6 jit_solution(2338002099792688461)
XLA Ops:
  0.6 50.8 %layer.1 = (bf16[32,2048]{1,0:T(8,128)(2,1)}, bf16[32,128]{1,0:T(8,128)(2,1)}, bf16[32,128]{1,0:T(8,128)(2,1)}) custom-call(bf16[32,2048]{1,0:T(8,128)(2,1)} %hidden_h.1, bf16[32,1024,128]{2,1,0:T(8,128)(2,1)} %keys_h.1, bf16[32,1024,128]{2,1,0:T(8,128)(2,1)} %values_h.1, s32[32]{0:T(128)} %lengths_h.1, f32[1,2048]{1,0:T(1,128)} %bitcast.5, ...), custom_call_target="tpu_custom_call" | custom-call | tf_op jit(solution)/shard_map/layer/pallas_call | solution.py:371
  51.5 1.6 %copy.23 = bf16[32,2048]{1,0:T(8,128)(2,1)} copy(bf16[32,2048]{1,0:T(8,128)(2,1)} %get-tuple-element.6) | data formatting | bytes 262144
  53.1 1.3 %copy.24 = bf16[32,128]{1,0:T(8,128)(2,1)} copy(bf16[32,128]{1,0:T(8,128)(2,1)} %get-tuple-element.7) | data formatting | bytes 16384
  54.4 1.3 %copy.25 = bf16[32,128]{1,0:T(8,128)(2,1)} copy(bf16[32,128]{1,0:T(8,128)(2,1)} %get-tuple-element.8) | data formatting | bytes 16384

commit v2 on v1

--- a/solution.py
+++ b/solution.py
@@ -51,11 +51,11 @@
 def kernel(
     hidden_h, keys_h, values_h, lengths_h, gain1_h, wq_h, wk_h, wv_h, mixing_h, hgain_h, wo_h, gain2_h,
     routes_h, rweight_h, gate_h, up_h, down_h,
-    out_h, nkey_h, nvalue_h,
+    out,
     hidden, kbuf, vbuf, lens, gain1, wq, wk, wv, mixing, hgain, wo, gain2, routes, rweight, wg, wu, wd,
-    qbuf, nkbuf, nvbuf, scores, contrast, heads, resid, outbuf, nkout, nvout,
+    qbuf, nkbuf, nvbuf, scores, contrast, heads, resid, picked,
     wcomb, sendbuf, recvbuf, ybuf, retbuf,
-    small_sem, wq_sem, k_sem, v_sem, wo_sem, exp_sem, out_sem,
+    small_sem, wq_sem, k_sem, v_sem, wo_sem, exp_sem,
     wsend_sem, wrecv_sem, dsend_sem, drecv_sem, rsend_sem, rrecv_sem,
 ):
     me = lax.axis_index("ep")
@@ -66,40 +66,28 @@
     cz = lax.div(chip, SIDE * SIDE)
     sibling = chip * 2 + (1 - core)
 
+    ahead_x = [lax.rem(cx + d, SIDE) * 2 + core for d in range(SIDE)]
+    ahead_y = [lax.rem(cy + d, SIDE) * (SIDE * 2) for d in range(SIDE)]
+    ahead_z = [lax.rem(cz + d, SIDE) * (SIDE * SIDE * 2) for d in range(SIDE)]
+
     def partner(k, sign):
-        rel = lax.rem(k * INV, CHIPS)
-        dx = lax.rem(rel, SIDE)
-        dy = lax.rem(lax.div(rel, SIDE), SIDE)
-        dz = lax.div(rel, SIDE * SIDE)
-        x = lax.rem(cx + sign * dx + SIDE, SIDE)
-        y = lax.rem(cy + sign * dy + SIDE, SIDE)
-        z = lax.rem(cz + sign * dz + SIDE, SIDE)
-        return ((z * SIDE + y) * SIDE + x) * 2 + core
-
-    barrier = pltpu.get_barrier_semaphore()
-
-    def greet(k, carry):
-        pl.semaphore_signal(barrier, inc=1, device_id=(partner(k, 1),), device_id_type=MESH)
-        return carry
-
-    lax.fori_loop(1, CHIPS, greet, 0)
-    pl.semaphore_signal(barrier, inc=1, device_id=(sibling,), device_id_type=MESH)
+        rel = k * INV % CHIPS
+        dx, dy, dz = rel % SIDE, rel // SIDE % SIDE, rel // (SIDE * SIDE)
+        return ahead_z[sign * dz % SIDE] + ahead_y[sign * dy % SIDE] + ahead_x[sign * dx % SIDE]
 
     smalls = [
-        (hidden_h, hidden), (gain1_h, gain1), (wk_h, wk), (wv_h, wv), (lengths_h, lens), (mixing_h, mixing),
-        (hgain_h, hgain), (gain2_h, gain2), (routes_h, routes), (rweight_h, rweight),
+        (routes_h, routes), (rweight_h, rweight), (hidden_h, hidden), (gain1_h, gain1), (lengths_h, lens),
+        (mixing_h, mixing), (hgain_h, hgain), (gain2_h, gain2), (wk_h, wk), (wv_h, wv),
     ]
     small = [pltpu.make_async_copy(a, b, small_sem.at[i]) for i, (a, b) in enumerate(smalls)]
-    small[0].start()
-    small[1].start()
+    for copy in small:
+        copy.start()
     step = D // WCHUNKS
     wq_copies = [
         pltpu.make_async_copy(wq_h.at[pl.ds(i * step, step)], wq.at[pl.ds(i * step, step)], wq_sem.at[i])
         for i in range(WCHUNKS)
     ]
     for copy in wq_copies:
-        copy.start()
-    for copy in small[2:]:
         copy.start()
 
     def fetch(g, carry):
@@ -115,35 +103,20 @@
         pltpu.make_async_copy(down_h.at[0], wd.at[core], exp_sem.at[2]),
     ]
     wo_copy = pltpu.make_async_copy(wo_h, wo, wo_sem)
-    fetch(0, 0)
+    lax.fori_loop(0, GROUPS - 1, fetch, 0)
+    wo_copy.start()
+    fetch(GROUPS - 1, 0)
     for copy in own:
         copy.start()
-    lax.fori_loop(1, GROUPS, fetch, 0)
-    wo_copy.start()
-
+
+    barrier = pltpu.get_barrier_semaphore()
+    for k in range(1, CHIPS):
+        pl.semaphore_signal(barrier, inc=1, device_id=(partner(k, 1),), device_id_type=MESH)
+    pl.semaphore_signal(barrier, inc=1, device_id=(sibling,), device_id_type=MESH)
+
+    lanes = PIECES * SEQS
     small[0].wait()
     small[1].wait()
-    values = hidden[...].astype(F32)
-    normed = (values * row_scale(values) * gain1[...]).astype(BF16)
-    query = jnp.zeros((SEQS, HEADS * 2 * DK), F32)
-    for i in range(WCHUNKS):
-        wq_copies[i].wait()
-        query += dot(normed[:, i * step : (i + 1) * step], wq[i * step : (i + 1) * step, :])
-    qbuf[...] = query.astype(BF16).astype(F32) * DK ** (-0.5)
-    for copy in small[2:]:
-        copy.wait()
-    new_key = dot(normed, wk[...]).astype(BF16)
-    new_value = dot(normed, wv[...]).astype(BF16)
-    nkout[...] = new_key
-    nvout[...] = new_value
-    nkbuf[...] = new_key.astype(F32)
-    nvbuf[...] = new_value.astype(F32)
-    key_copy = pltpu.make_async_copy(nkout, nkey_h, out_sem.at[0])
-    value_copy = pltpu.make_async_copy(nvout, nvalue_h, out_sem.at[1])
-    key_copy.start()
-    value_copy.start()
-
-    lanes = PIECES * SEQS
     spread = (iota((SEQS, lanes), 0) == lax.rem(iota((SEQS, lanes), 1), SEQS)).astype(BF16)
     picks = dot(routes[...].astype(F32).astype(BF16), spread).astype(jnp.int32)
     lowest = jnp.min(picks, axis=0, keepdims=True)
@@ -172,10 +145,26 @@
         pick = jnp.where(hit, 1.0, pick)
         comb_high = jnp.where(hit, high[k : k + 1, :], comb_high)
         comb_low = jnp.where(hit, low[k : k + 1, :], comb_low)
-    pick = pick.astype(BF16)
+    picked[...] = pick.astype(BF16)
     wcomb[...] = jnp.transpose(jnp.concatenate([comb_high, comb_low], axis=1)).astype(BF16)
 
-    pl.semaphore_wait(barrier, CHIPS)
+    small[2].wait()
+    small[3].wait()
+    values = hidden[...].astype(F32)
+    normed = (values * row_scale(values) * gain1[...]).astype(BF16)
+    query = jnp.zeros((SEQS, HEADS * 2 * DK), F32)
+    for i in range(WCHUNKS):
+        wq_copies[i].wait()
+        query += dot(normed[:, i * step : (i + 1) * step], wq[i * step : (i + 1) * step, :])
+    qbuf[...] = query.astype(BF16).astype(F32) * DK ** (-0.5)
+    for copy in small[4:]:
+        copy.wait()
+    new_key = dot(normed, wk[...]).astype(BF16)
+    new_value = dot(normed, wv[...]).astype(BF16)
+    out[:, D : D + 2 * DK] = new_key
+    out[:, D + 2 * DK :] = new_value
+    nkbuf[...] = new_key.astype(F32)
+    nvbuf[...] = new_value.astype(F32)
 
     def share(source, index):
         return pltpu.make_async_remote_copy(
@@ -235,14 +224,6 @@
         normal = mixed * row_scale(mixed) * hgain[...]
         for h in range(HEADS):
             heads[pl.ds(first, GROUP), h * DV : (h + 1) * DV] = normal[h * GROUP : (h + 1) * GROUP]
-
-        @pl.when(g == 0)
-        def _():
-            for copy in own:
-                copy.wait()
-            for i, ref in enumerate((wg, wu, wd)):
-                share(ref, i).start()
-
         return carry
 
     lax.fori_loop(0, GROUPS, attend, 0)
@@ -254,21 +235,20 @@
     resid[...] = values
     given = values * row_scale(values) * gain2[...]
     stacked = jnp.concatenate([given[:, c * WIDTH : (c + 1) * WIDTH] for c in range(PIECES)], axis=0).astype(BF16)
-    packed = dot(pick, stacked).astype(BF16).reshape(CHIPS, ROWS, WIDTH)
+    packed = dot(picked[...], stacked).astype(BF16).reshape(CHIPS, ROWS, WIDTH)
     sendbuf[...] = packed
-    recvbuf[0] = sendbuf[0]
-
-    def dispatch(k, carry):
+
+    pl.semaphore_wait(barrier, CHIPS)
+    for k in range(1, CHIPS):
         pltpu.make_async_remote_copy(
-            src_ref=sendbuf.at[k], dst_ref=recvbuf.at[k], send_sem=dsend_sem, recv_sem=drecv_sem.at[lax.div(k, PER)],
+            src_ref=sendbuf.at[k], dst_ref=recvbuf.at[k], send_sem=dsend_sem, recv_sem=drecv_sem.at[k // PER],
             device_id=(partner(k, 1),), device_id_type=MESH,
         ).start()
-        return carry
-
-    lax.fori_loop(1, CHIPS, dispatch, 0)
-
+    for copy in own:
+        copy.wait()
     for i, ref in enumerate((wg, wu, wd)):
-        share(ref, i).wait()
+        share(ref, i).start()
+    recvbuf[0] = sendbuf[0]
 
     size = PER * ROWS
     line = iota((size, size), 0)
@@ -281,7 +261,7 @@
     to_messages = (shuffled(line) == column).astype(BF16)
     tall = PER * CAP
 
-    def expert(b, carry):
+    def expert(b):
         pieces = dot(to_pieces, recvbuf[pl.ds(b * PER, PER)].reshape(size, WIDTH)).astype(BF16)
         inner = []
         for j in range(2):
@@ -297,49 +277,49 @@
             cut = slice(c * WIDTH, (c + 1) * WIDTH)
             result.append((dot(inner[0], wd[0, :, cut]) + dot(inner[1], wd[1, :, cut])).astype(BF16))
         ybuf[pl.ds(b * PER, PER)] = dot(to_messages, jnp.concatenate(result, axis=0)).astype(BF16).reshape(PER, ROWS, WIDTH)
-
-        def give(k, inside):
+        for k in range(max(b * PER, 1), (b + 1) * PER):
             pltpu.make_async_remote_copy(
                 src_ref=ybuf.at[k], dst_ref=retbuf.at[k], send_sem=rsend_sem, recv_sem=rrecv_sem.at[b],
                 device_id=(partner(k, -1),), device_id_type=MESH,
             ).start()
-            return inside
-
-        lax.fori_loop(jnp.maximum(b * PER, 1), (b + 1) * PER, give, 0)
-        return carry
 
     def landed(ref, first, count, sem):
         part = ref.at[pl.ds(first, count)]
         pltpu.make_async_copy(part, part, sem).wait()
 
-    landed(recvbuf, 1, PER - 1, drecv_sem.at[0])
-    expert(0, 0)
+    def wait_block(ref, b, sem):
+        landed(ref, max(b * PER, 1), PER - (b == 0), sem.at[b])
+
+    for b in range(BLOCKS):
+        wait_block(recvbuf, b, drecv_sem)
+        if b == 0:
+            for i, ref in enumerate((wg, wu, wd)):
+                share(ref, i).wait()
+        expert(b)
     retbuf[0] = ybuf[0]
-
-    def later(b, carry):
-        landed(recvbuf, b * PER, PER, drecv_sem.at[b])
-        return expert(b, carry)
-
-    lax.fori_loop(1, BLOCKS, later, 0)
 
     total = jnp.zeros((2 * lanes, WIDTH), F32)
     for b in range(BLOCKS):
-        if b == 0:
-            landed(retbuf, 1, PER - 1, rrecv_sem.at[0])
-        else:
-            landed(retbuf, b * PER, PER, rrecv_sem.at[b])
+        wait_block(retbuf, b, rrecv_sem)
         total += dot(wcomb[:, b * size : (b + 1) * size], retbuf[b * PER : (b + 1) * PER].reshape(size, WIDTH))
     routed = total[:lanes] + total[lanes:]
     for c in range(PIECES):
         cut = slice(c * WIDTH, (c + 1) * WIDTH)
-        outbuf[:, cut] = (resid[:, cut] + routed[c * SEQS : (c + 1) * SEQS]).astype(BF16)
-    out_copy = pltpu.make_async_copy(outbuf, out_h, out_sem.at[2])
-    out_copy.start()
+        out[:, cut] = (resid[:, cut] + routed[c * SEQS : (c + 1) * SEQS]).astype(BF16)
     landed(sendbuf, 1, CHIPS - 1, dsend_sem)
     landed(ybuf, 1, CHIPS - 1, rsend_sem)
-    key_copy.wait()
-    value_copy.wait()
-    out_copy.wait()
+
+
+def finish(packed, out, new_key, new_value, sem):
+    copies = [
+        pltpu.make_async_copy(packed.at[:, pl.ds(0, D)], out, sem.at[0]),
+        pltpu.make_async_copy(packed.at[:, pl.ds(D, 2 * DK)], new_key, sem.at[1]),
+        pltpu.make_async_copy(packed.at[:, pl.ds(D + 2 * DK, DV)], new_value, sem.at[2]),
+    ]
+    for copy in copies:
+        copy.start()
+    for copy in copies:
+        copy.wait()
 
 
 def per_device(
@@ -361,28 +341,37 @@
         vmem((2, D, PART), BF16), vmem((2, D, PART), BF16), vmem((2, PART, D), BF16),
         vmem((SEQS, HEADS * 2 * DK), F32), vmem((SEQS, 2 * DK), F32), vmem((SEQS, DV), F32),
         vmem((SPAN, LANES), F32), vmem((SPAN, LANES), BF16), vmem((SEQS, HEADS * DV), F32), vmem((SEQS, D), F32),
-        vmem((SEQS, D), BF16), vmem((SEQS, 2 * DK), BF16), vmem((SEQS, DV), BF16),
+        vmem((CHIPS * ROWS, PIECES * SEQS), BF16),
         vmem((2 * PIECES * SEQS, CHIPS * ROWS), BF16),
         vmem((CHIPS, ROWS, WIDTH), BF16), vmem((CHIPS, ROWS, WIDTH), BF16),
         vmem((CHIPS, ROWS, WIDTH), BF16), vmem((CHIPS, ROWS, WIDTH), BF16),
-        sem((10,)), sem((WCHUNKS,)), sem((GROUPS,)), sem((GROUPS,)), sem, sem((3,)), sem((3,)),
+        sem((10,)), sem((WCHUNKS,)), sem((GROUPS,)), sem((GROUPS,)), sem, sem((3,)),
         sem((3,)), sem((3,)), sem, sem((BLOCKS,)), sem, sem((BLOCKS,)),
     ]
+    packed = pl.pallas_call(
+        kernel,
+        out_shape=pltpu.VMEM((SEQS, D + 2 * DK + DV), BF16),
+        in_specs=[pl.BlockSpec(memory_space=pltpu.HBM)] * len(args),
+        out_specs=pl.BlockSpec(memory_space=pltpu.VMEM),
+        scratch_shapes=scratch,
+        compiler_params=pltpu.CompilerParams(
+            collective_id=0, has_side_effects=True, vmem_limit_bytes=62 * 1024 * 1024
+        ),
+        name="layer",
+    )(*args)
     return pl.pallas_call(
-        kernel,
+        finish,
         out_shape=(
             jax.ShapeDtypeStruct((SEQS, D), BF16),
             jax.ShapeDtypeStruct((SEQS, 2 * DK), BF16),
             jax.ShapeDtypeStruct((SEQS, DV), BF16),
         ),
-        in_specs=[pl.BlockSpec(memory_space=pl.ANY)] * len(args),
-        out_specs=[pl.BlockSpec(memory_space=pl.ANY)] * 3,
-        scratch_shapes=scratch,
-        compiler_params=pltpu.CompilerParams(
-            collective_id=0, has_side_effects=True, vmem_limit_bytes=60 * 1024 * 1024
-        ),
-        name="layer",
-    )(*args)
+        in_specs=[pl.BlockSpec(memory_space=pltpu.VMEM)],
+        out_specs=[pl.BlockSpec(memory_space=pltpu.HBM)] * 3,
+        scratch_shapes=[sem((3,))],
+        compiler_params=pltpu.CompilerParams(vmem_limit_bytes=8 * 1024 * 1024),
+        name="finish",
+    )(packed)
 
 
 def solution(mesh):

time: 55.9 us -> 48.3 us (0.86)
  local copies, waits for them, and re-layouts: 4.16 us -> 0 us
  Pallas kernels: 50.8 us -> 47.5 us
    unnamed x3 -> x0, local copies, waits for them, and re-layouts: 4.16 us -> none
    pallas_call x1 -> x2, Pallas kernels: 50.8 us -> 47.5 us  [the longest x1 46.9 us: per_device(): pl.pallas_call(kernel, out_shape=pltpu.VMEM((SEQS, D + 2 * DK + DV), BF16...]
where the time goes in v2:
time: 48.3 us; the launch traced here: 48.2 us
  Pallas kernels  47.5 us (98%)
  between operations  0.65 us (1%)
    pallas_call x1, Pallas kernels, per_device(): pl.pallas_call(kernel, out_shape=pltpu.VMEM((SEQS, D + 2 * DK + DV), BF16...  46.9 us

profile of v2, /device:TPU:0, one launch (start us, length us, event | category | flops | bytes accessed | tf_op | source)
XLA Modules:
  0.0 48.2 jit_solution(10684838119956046262)
XLA Ops:
  0.6 46.9 %layer.1.packed = bf16[32,2304]{1,0:T(8,128)(2,1)S(1)} custom-call(bf16[32,2048]{1,0:T(8,128)(2,1)} %hidden_h.1, bf16[32,1024,128]{2,1,0:T(8,128)(2,1)} %keys_h.1, bf16[32,1024,128]{2,1,0:T(8,128)(2,1)} %values_h.1, s32[32]{0:T(128)} %lengths_h.1, f32[1,2048]{1,0:T(1,128)} %bitcast.5, bf16[2048,1024]{1,0:T(8,128)(2,1)} %wq_h.1, bf16[2048,128]{1,0:T(8,128)(2,1)} %wk_h.1, ...), custom_call_target="tpu_custom_call" | custom-call | tf_op jit(solution)/shard_map/layer/pallas_call | solution.py:351
  47.5 0.7 %finish.1 = (bf16[32,2048]{1,0:T(8,128)(2,1)}, bf16[32,128]{1,0:T(8,128)(2,1)}, bf16[32,128]{1,0:T(8,128)(2,1)}) custom-call(bf16[32,2304]{1,0:T(8,128)(2,1)S(1)} %layer.1.packed), custom_call_target="tpu_custom_call" | custom-call | tf_op jit(solution)/shard_map/finish/pallas_call | solution.py:362

commit v3 on v2

--- a/solution.py
+++ b/solution.py
@@ -22,7 +22,7 @@
 CAP = 4
 CHIPS = 64
 SIDE = 4
-GROUP = 8
+GROUP = 16
 GROUPS = SEQS // GROUP
 WCHUNKS = 4
 PIECES = 2
@@ -30,9 +30,10 @@
 ROWS = CAP * PIECES
 BLOCKS = 4
 PER = CHIPS // BLOCKS
-MUL = 37
+MUL = 45
 INV = pow(MUL, -1, CHIPS)
-LANES = GROUP * HEADS * 2
+LANES = GROUP * HEADS
+CUT = 128
 EPS = 1e-06
 
 
@@ -53,7 +54,7 @@
     routes_h, rweight_h, gate_h, up_h, down_h,
     out,
     hidden, kbuf, vbuf, lens, gain1, wq, wk, wv, mixing, hgain, wo, gain2, routes, rweight, wg, wu, wd,
-    qbuf, nkbuf, nvbuf, scores, contrast, heads, resid, picked,
+    qbuf, nkbuf, nvbuf, diag, scores, contrast, heads, resid, picked,
     wcomb, sendbuf, recvbuf, ybuf, retbuf,
     small_sem, wq_sem, k_sem, v_sem, wo_sem, exp_sem,
     wsend_sem, wrecv_sem, dsend_sem, drecv_sem, rsend_sem, rrecv_sem,
@@ -90,12 +91,13 @@
     for copy in wq_copies:
         copy.start()
 
-    def fetch(g, carry):
-        for s in range(GROUP):
-            pltpu.make_async_copy(keys_h.at[g * GROUP + s], kbuf.at[g, :, pl.ds(s * 2 * DK, 2 * DK)], k_sem.at[g]).start()
-        for s in range(GROUP):
-            pltpu.make_async_copy(values_h.at[g * GROUP + s], vbuf.at[g, :, pl.ds(s * DV, DV)], v_sem.at[g]).start()
-        return carry
+    def fetch_keys(g):
+        part = pl.ds(g * GROUP, GROUP)
+        pltpu.make_async_copy(keys_h.at[part], kbuf.at[part], k_sem.at[g]).start()
+
+    def fetch_values(g):
+        part = pl.ds(g * GROUP, GROUP)
+        pltpu.make_async_copy(values_h.at[part], vbuf.at[part], v_sem.at[g]).start()
 
     own = [
         pltpu.make_async_copy(gate_h.at[0], wg.at[core], exp_sem.at[0]),
@@ -103,11 +105,10 @@
         pltpu.make_async_copy(down_h.at[0], wd.at[core], exp_sem.at[2]),
     ]
     wo_copy = pltpu.make_async_copy(wo_h, wo, wo_sem)
-    lax.fori_loop(0, GROUPS - 1, fetch, 0)
-    wo_copy.start()
-    fetch(GROUPS - 1, 0)
-    for copy in own:
-        copy.start()
+
+    def fetch_own():
+        for copy in own:
+            copy.start()
 
     barrier = pltpu.get_barrier_semaphore()
     for k in range(1, CHIPS):
@@ -148,6 +149,7 @@
     picked[...] = pick.astype(BF16)
     wcomb[...] = jnp.transpose(jnp.concatenate([comb_high, comb_low], axis=1)).astype(BF16)
 
+    fetch_keys(0)
     small[2].wait()
     small[3].wait()
     values = hidden[...].astype(F32)
@@ -166,6 +168,8 @@
     nkbuf[...] = new_key.astype(F32)
     nvbuf[...] = new_value.astype(F32)
 
+    fetch_values(0)
+
     def share(source, index):
         return pltpu.make_async_remote_copy(
             src_ref=source.at[core], dst_ref=source.at[core], send_sem=wsend_sem.at[index],
@@ -174,59 +178,75 @@
 
     lane = iota((1, LANES), 1)
     lane_seq = lax.rem(lane, GROUP)
-    lane_head = lax.rem(lax.div(lane, GROUP), HEADS)
     mix = jnp.zeros((1, LANES), F32)
     for h in range(HEADS):
-        mix = jnp.where(lane_head == h, mixing[h], mix)
-    mix = jnp.where(lane < LANES // 2, 1.0, mix)
-    row = iota((LANES, 2 * DK), 0)
-    col = iota((LANES, 2 * DK), 1)
-    same_map = lax.div(row, LANES // 2) == lax.div(col, DK)
-    row_seq = lax.rem(row, GROUP)
-
-    def attend(g, carry):
-        first = pl.multiple_of(g * GROUP, GROUP)
-        rows = [qbuf[pl.ds(first, GROUP), h * 2 * DK : (h + 1) * 2 * DK] for h in range(HEADS)]
-        block = jnp.concatenate(rows + rows, axis=0)
-        block = jnp.where(same_map, block, 0.0)
-        diag = jnp.concatenate(
-            [jnp.where(row_seq == s, block, 0.0).astype(BF16) for s in range(GROUP)], axis=1
-        )
+        mix = jnp.where(lax.div(lane, GROUP) == h, mixing[h], mix)
+    row_seq = lax.rem(iota((LANES, DV), 0), GROUP)
+    blank = jnp.zeros((DK, LANES), BF16)
+
+    def attend(g, with_keys, with_values):
+        first = g * GROUP
+        block = jnp.concatenate(
+            [qbuf[pl.ds(first, GROUP), h * 2 * DK : (h + 1) * 2 * DK] for h in range(HEADS)], axis=0
+        ).T
+        fresh = jnp.concatenate([nkbuf[pl.ds(first, GROUP), :]] * HEADS, axis=0).T
         limit = jnp.zeros((1, LANES), jnp.int32)
         for s in range(GROUP):
             limit = jnp.where(lane_seq == s, lens[g * GROUP + s], limit)
-        fresh = nkbuf[pl.ds(first, GROUP), :]
-        fresh_rows = jnp.concatenate(
-            [jnp.where(iota((GROUP, 2 * DK), 0) == s, fresh, 0.0).astype(BF16) for s in range(GROUP)], axis=1
+            one = jnp.where(lane_seq == s, block, 0.0).astype(BF16)
+            for m in range(2):
+                for half in range(2):
+                    diag[s * 2 * DK + half * DK : s * 2 * DK + (half + 1) * DK, m * LANES : (m + 1) * LANES] = (
+                        one[half * DK : (half + 1) * DK] if half == m else blank
+                    )
+        both = block * fresh
+        own_score = jnp.concatenate(
+            [jnp.sum(both[m * DK : (m + 1) * DK], axis=0, keepdims=True) for m in range(2)], axis=1
         )
-        own_score = jnp.sum(dot(fresh_rows, diag, ((1,), (1,))), axis=0, keepdims=True)
-        pltpu.make_async_copy(kbuf.at[g], kbuf.at[g], k_sem.at[g]).wait()
-        score = dot(kbuf[g], diag, ((1,), (1,)))
-        score = jnp.where(iota((SPAN, LANES), 0) < limit, score, -jnp.inf)
+        limit = jnp.concatenate([limit, limit], axis=1)
+        pltpu.make_async_copy(keys_h.at[pl.ds(first, GROUP)], kbuf.at[pl.ds(first, GROUP)], k_sem.at[g]).wait()
+        with_keys()
+        score = jnp.zeros((SPAN, 2 * LANES), F32)
+        for s in range(0, GROUP, 2):
+            pair = jnp.concatenate([kbuf[first + s], kbuf[first + s + 1]], axis=1)
+            score += dot(pair, diag[s * 2 * DK : (s + 2) * 2 * DK])
+        score = jnp.where(iota((SPAN, 2 * LANES), 0) < limit, score, -jnp.inf)
         scores[...] = score
         highest = jnp.maximum(jnp.max(score, axis=0, keepdims=True), own_score)
-        weight = jnp.exp(scores[...] - highest)
-        scores[...] = weight
         own_weight = jnp.exp(own_score - highest)
-        total = jnp.sum(weight, axis=0, keepdims=True) + own_weight
-        factor = mix / total
-        part = scores[...] * factor
-        contrast[...] = (part - pltpu.roll(part, LANES // 2, 1)).astype(BF16)
+        total = own_weight
+        for c in range(0, SPAN, CUT):
+            weight = jnp.exp(scores[c : c + CUT] - highest)
+            scores[c : c + CUT] = weight
+            total += jnp.sum(weight, axis=0, keepdims=True)
+        factor = jnp.concatenate([jnp.ones((1, LANES), F32), mix], axis=1) / total
+        for c in range(0, SPAN, CUT):
+            part = scores[c : c + CUT] * factor
+            contrast[:, c : c + CUT] = (part[:, :LANES] - part[:, LANES:]).T.astype(BF16)
         own_part = own_weight * factor
-        own_contrast = own_part - pltpu.roll(own_part, LANES // 2, 1)
-        pltpu.make_async_copy(vbuf.at[g], vbuf.at[g], v_sem.at[g]).wait()
-        full = dot(contrast[...], vbuf[g], ((0,), (0,)))[: LANES // 2]
-        own_rows = jnp.where(iota((GROUP, LANES), 0) == lane_seq, own_contrast, 0.0).astype(BF16)
-        mixed = dot(own_rows, nvbuf[pl.ds(first, GROUP), :].astype(BF16), ((0,), (0,)))[: LANES // 2]
-        out_seq = lax.rem(iota((LANES // 2, DV), 0), GROUP)
-        for s in range(GROUP):
-            mixed += jnp.where(out_seq == s, full[:, s * DV : (s + 1) * DV], 0.0)
+        own_contrast = (own_part[:, :LANES] - own_part[:, LANES:]).astype(BF16).astype(F32)
+        own_rows = jnp.broadcast_to(own_contrast, (DV, LANES)).T
+        mixed = own_rows * jnp.concatenate([nvbuf[pl.ds(first, GROUP), :]] * HEADS, axis=0)
+        pltpu.make_async_copy(values_h.at[pl.ds(first, GROUP)], vbuf.at[pl.ds(first, GROUP)], v_sem.at[g]).wait()
+        with_values()
+        for s in range(0, GROUP, 2):
+            pair = dot(contrast[...], jnp.concatenate([vbuf[first + s], vbuf[first + s + 1]], axis=1))
+            mixed += jnp.where(row_seq == s, pair[:, :DV], 0.0) + jnp.where(row_seq == s + 1, pair[:, DV:], 0.0)
         normal = mixed * row_scale(mixed) * hgain[...]
         for h in range(HEADS):
             heads[pl.ds(first, GROUP), h * DV : (h + 1) * DV] = normal[h * GROUP : (h + 1) * GROUP]
-        return carry
-
-    lax.fori_loop(0, GROUPS, attend, 0)
+
+    def with_first_keys():
+        fetch_own()
+        fetch_keys(1)
+
+    attend(0, with_first_keys, functools.partial(fetch_values, 1))
+    pl.semaphore_wait(barrier, CHIPS)
+    for copy in own:
+        copy.wait()
+    for i, ref in enumerate((wg, wu, wd)):
+        share(ref, i).start()
+    attend(1, wo_copy.start, lambda: None)
 
     wo_copy.wait()
     update = dot(heads[...].astype(BF16), wo[...])
@@ -238,16 +258,11 @@
     packed = dot(picked[...], stacked).astype(BF16).reshape(CHIPS, ROWS, WIDTH)
     sendbuf[...] = packed
 
-    pl.semaphore_wait(barrier, CHIPS)
     for k in range(1, CHIPS):
         pltpu.make_async_remote_copy(
             src_ref=sendbuf.at[k], dst_ref=recvbuf.at[k], send_sem=dsend_sem, recv_sem=drecv_sem.at[k // PER],
             device_id=(partner(k, 1),), device_id_type=MESH,
         ).start()
-    for copy in own:
-        copy.wait()
-    for i, ref in enumerate((wg, wu, wd)):
-        share(ref, i).start()
     recvbuf[0] = sendbuf[0]
 
     size = PER * ROWS
@@ -334,13 +349,13 @@
     vmem = pltpu.VMEM
     sem = pltpu.SemaphoreType.DMA
     scratch = [
-        vmem((SEQS, D), BF16), vmem((GROUPS, SPAN, GROUP * 2 * DK), BF16), vmem((GROUPS, SPAN, GROUP * DV), BF16),
+        vmem((SEQS, D), BF16), vmem((SEQS, SPAN, 2 * DK), BF16), vmem((SEQS, SPAN, DV), BF16),
         pltpu.SMEM((SEQS,), jnp.int32), vmem((1, D), F32), vmem((D, HEADS * 2 * DK), BF16), vmem((D, 2 * DK), BF16),
         vmem((D, DV), BF16), pltpu.SMEM((HEADS,), F32), vmem((1, DV), F32), vmem((HEADS * DV, D), BF16),
         vmem((1, D), F32), vmem((TOP_K, SEQS), jnp.int32), vmem((TOP_K, SEQS), F32),
         vmem((2, D, PART), BF16), vmem((2, D, PART), BF16), vmem((2, PART, D), BF16),
         vmem((SEQS, HEADS * 2 * DK), F32), vmem((SEQS, 2 * DK), F32), vmem((SEQS, DV), F32),
-        vmem((SPAN, LANES), F32), vmem((SPAN, LANES), BF16), vmem((SEQS, HEADS * DV), F32), vmem((SEQS, D), F32),
+        vmem((GROUP * 2 * DK, 2 * LANES), BF16), vmem((SPAN, 2 * LANES), F32), vmem((LANES, SPAN), BF16), vmem((SEQS, HEADS * DV), F32), vmem((SEQS, D), F32),
         vmem((CHIPS * ROWS, PIECES * SEQS), BF16),
         vmem((2 * PIECES * SEQS, CHIPS * ROWS), BF16),
         vmem((CHIPS, ROWS, WIDTH), BF16), vmem((CHIPS, ROWS, WIDTH), BF16),

time: 48.3 us -> 46.5 us (0.963)
  Pallas kernels: 47.5 us -> 45.7 us
    pallas_call x1, Pallas kernels: 46.9 us -> 45.1 us  [per_device(): pl.pallas_call(kernel, out_shape=pltpu.VMEM((SEQS, D + 2 * DK + DV), BF16...]
where the time goes in v3:
time: 46.5 us; the launch traced here: 46.4 us
  Pallas kernels  45.7 us (98%)
  between operations  0.65 us (1%)
    pallas_call x1, Pallas kernels, per_device(): pl.pallas_call(kernel, out_shape=pltpu.VMEM((SEQS, D + 2 * DK + DV), BF16...  45.1 us

profile of v3, /device:TPU:0, one launch (start us, length us, event | category | flops | bytes accessed | tf_op | source)
XLA Modules:
  0.0 46.4 jit_solution(1417672792066409052)
XLA Ops:
  0.6 45.1 %layer.1.packed = bf16[32,2304]{1,0:T(8,128)(2,1)S(1)} custom-call(bf16[32,2048]{1,0:T(8,128)(2,1)} %hidden_h.1, bf16[32,1024,128]{2,1,0:T(8,128)(2,1)} %keys_h.1, bf16[32,1024,128]{2,1,0:T(8,128)(2,1)} %values_h.1, s32[32]{0:T(128)} %lengths_h.1, f32[1,2048]{1,0:T(1,128)} %bitcast.5, bf16[2048,1024]{1,0:T(8,128)(2,1)} %wq_h.1, bf16[2048,128]{1,0:T(8,128)(2,1)} %wk_h.1, ...), custom_call_target="tpu_custom_call" | custom-call | tf_op jit(solution)/shard_map/layer/pallas_call | solution.py:366
  45.7 0.7 %finish.1 = (bf16[32,2048]{1,0:T(8,128)(2,1)}, bf16[32,128]{1,0:T(8,128)(2,1)}, bf16[32,128]{1,0:T(8,128)(2,1)}) custom-call(bf16[32,2304]{1,0:T(8,128)(2,1)S(1)} %layer.1.packed), custom_call_target="tpu_custom_call" | custom-call | tf_op jit(solution)/shard_map/finish/pallas_call | solution.py:377

commit v4 on v3

--- a/solution.py
+++ b/solution.py
@@ -168,7 +168,7 @@
     nkbuf[...] = new_key.astype(F32)
     nvbuf[...] = new_value.astype(F32)
 
-    fetch_values(0)
+    fetch_keys(1)
 
     def share(source, index):
         return pltpu.make_async_remote_copy(
@@ -184,7 +184,7 @@
     row_seq = lax.rem(iota((LANES, DV), 0), GROUP)
     blank = jnp.zeros((DK, LANES), BF16)
 
-    def attend(g, with_keys, with_values):
+    def prepare(g):
         first = g * GROUP
         block = jnp.concatenate(
             [qbuf[pl.ds(first, GROUP), h * 2 * DK : (h + 1) * 2 * DK] for h in range(HEADS)], axis=0
@@ -196,57 +196,70 @@
             one = jnp.where(lane_seq == s, block, 0.0).astype(BF16)
             for m in range(2):
                 for half in range(2):
-                    diag[s * 2 * DK + half * DK : s * 2 * DK + (half + 1) * DK, m * LANES : (m + 1) * LANES] = (
+                    diag[g, s * 2 * DK + half * DK : s * 2 * DK + (half + 1) * DK, m * LANES : (m + 1) * LANES] = (
                         one[half * DK : (half + 1) * DK] if half == m else blank
                     )
         both = block * fresh
         own_score = jnp.concatenate(
             [jnp.sum(both[m * DK : (m + 1) * DK], axis=0, keepdims=True) for m in range(2)], axis=1
         )
-        limit = jnp.concatenate([limit, limit], axis=1)
+        return jnp.concatenate([limit, limit], axis=1), own_score
+
+    def compare(g, limit, own_score):
+        first = g * GROUP
         pltpu.make_async_copy(keys_h.at[pl.ds(first, GROUP)], kbuf.at[pl.ds(first, GROUP)], k_sem.at[g]).wait()
-        with_keys()
         score = jnp.zeros((SPAN, 2 * LANES), F32)
         for s in range(0, GROUP, 2):
             pair = jnp.concatenate([kbuf[first + s], kbuf[first + s + 1]], axis=1)
-            score += dot(pair, diag[s * 2 * DK : (s + 2) * 2 * DK])
+            score += dot(pair, diag[g, s * 2 * DK : (s + 2) * 2 * DK])
         score = jnp.where(iota((SPAN, 2 * LANES), 0) < limit, score, -jnp.inf)
-        scores[...] = score
-        highest = jnp.maximum(jnp.max(score, axis=0, keepdims=True), own_score)
+        scores[g] = score
+        return jnp.maximum(jnp.max(score, axis=0, keepdims=True), own_score)
+
+    def soften(g, highest, own_score):
         own_weight = jnp.exp(own_score - highest)
         total = own_weight
         for c in range(0, SPAN, CUT):
-            weight = jnp.exp(scores[c : c + CUT] - highest)
-            scores[c : c + CUT] = weight
+            weight = jnp.exp(scores[g, c : c + CUT] - highest)
+            scores[g, c : c + CUT] = weight
             total += jnp.sum(weight, axis=0, keepdims=True)
         factor = jnp.concatenate([jnp.ones((1, LANES), F32), mix], axis=1) / total
         for c in range(0, SPAN, CUT):
-            part = scores[c : c + CUT] * factor
-            contrast[:, c : c + CUT] = (part[:, :LANES] - part[:, LANES:]).T.astype(BF16)
+            part = scores[g, c : c + CUT] * factor
+            contrast[g, :, c : c + CUT] = (part[:, :LANES] - part[:, LANES:]).T.astype(BF16)
         own_part = own_weight * factor
-        own_contrast = (own_part[:, :LANES] - own_part[:, LANES:]).astype(BF16).astype(F32)
+        return (own_part[:, :LANES] - own_part[:, LANES:]).astype(BF16).astype(F32)
+
+    def gather(g, own_contrast):
+        first = g * GROUP
         own_rows = jnp.broadcast_to(own_contrast, (DV, LANES)).T
         mixed = own_rows * jnp.concatenate([nvbuf[pl.ds(first, GROUP), :]] * HEADS, axis=0)
-        pltpu.make_async_copy(values_h.at[pl.ds(first, GROUP)], vbuf.at[pl.ds(first, GROUP)], v_sem.at[g]).wait()
-        with_values()
         for s in range(0, GROUP, 2):
-            pair = dot(contrast[...], jnp.concatenate([vbuf[first + s], vbuf[first + s + 1]], axis=1))
+            pair = dot(contrast[g], jnp.concatenate([vbuf[first + s], vbuf[first + s + 1]], axis=1))
             mixed += jnp.where(row_seq == s, pair[:, :DV], 0.0) + jnp.where(row_seq == s + 1, pair[:, DV:], 0.0)
         normal = mixed * row_scale(mixed) * hgain[...]
         for h in range(HEADS):
             heads[pl.ds(first, GROUP), h * DV : (h + 1) * DV] = normal[h * GROUP : (h + 1) * GROUP]
 
-    def with_first_keys():
-        fetch_own()
-        fetch_keys(1)
-
-    attend(0, with_first_keys, functools.partial(fetch_values, 1))
+    def await_values(g):
+        part = pl.ds(g * GROUP, GROUP)
+        pltpu.make_async_copy(values_h.at[part], vbuf.at[part], v_sem.at[g]).wait()
+
+    limit_a, own_a = prepare(0)
+    limit_b, own_b = prepare(1)
+    highest_a = compare(0, limit_a, own_a)
+    fetch_values(0)
+    fetch_values(1)
+    highest_b = compare(1, limit_b, own_b)
+    wo_copy.start()
+    fetch_own()
+    fresh_a = soften(0, highest_a, own_a)
+    await_values(0)
+    gather(0, fresh_a)
+    fresh_b = soften(1, highest_b, own_b)
+    await_values(1)
+    gather(1, fresh_b)
     pl.semaphore_wait(barrier, CHIPS)
-    for copy in own:
-        copy.wait()
-    for i, ref in enumerate((wg, wu, wd)):
-        share(ref, i).start()
-    attend(1, wo_copy.start, lambda: None)
 
     wo_copy.wait()
     update = dot(heads[...].astype(BF16), wo[...])
@@ -263,6 +276,10 @@
             src_ref=sendbuf.at[k], dst_ref=recvbuf.at[k], send_sem=dsend_sem, recv_sem=drecv_sem.at[k // PER],
             device_id=(partner(k, 1),), device_id_type=MESH,
         ).start()
+    for copy in own:
+        copy.wait()
+    for i, ref in enumerate((wg, wu, wd)):
+        share(ref, i).start()
     recvbuf[0] = sendbuf[0]
 
     size = PER * ROWS
@@ -355,7 +372,8 @@
         vmem((1, D), F32), vmem((TOP_K, SEQS), jnp.int32), vmem((TOP_K, SEQS), F32),
         vmem((2, D, PART), BF16), vmem((2, D, PART), BF16), vmem((2, PART, D), BF16),
         vmem((SEQS, HEADS * 2 * DK), F32), vmem((SEQS, 2 * DK), F32), vmem((SEQS, DV), F32),
-        vmem((GROUP * 2 * DK, 2 * LANES), BF16), vmem((SPAN, 2 * LANES), F32), vmem((LANES, SPAN), BF16), vmem((SEQS, HEADS * DV), F32), vmem((SEQS, D), F32),
+        vmem((GROUPS, GROUP * 2 * DK, 2 * LANES), BF16), vmem((GROUPS, SPAN, 2 * LANES), F32),
+        vmem((GROUPS, LANES, SPAN), BF16), vmem((SEQS, HEADS * DV), F32), vmem((SEQS, D), F32),
         vmem((CHIPS * ROWS, PIECES * SEQS), BF16),
         vmem((2 * PIECES * SEQS, CHIPS * ROWS), BF16),
         vmem((CHIPS, ROWS, WIDTH), BF16), vmem((CHIPS, ROWS, WIDTH), BF16),

time: 46.5 us -> 44.9 us (0.966)
  Pallas kernels: 45.7 us -> 44.1 us
    pallas_call x1, Pallas kernels: 45.1 us -> 43.4 us  [per_device(): pl.pallas_call(kernel, out_shape=pltpu.VMEM((SEQS, D + 2 * DK + DV), BF16...]
where the time goes in v4:
time: 44.9 us; the launch traced here: 44.8 us
  Pallas kernels  44.1 us (98%)
  between operations  0.65 us (1%)
    pallas_call x1, Pallas kernels, per_device(): pl.pallas_call(kernel, out_shape=pltpu.VMEM((SEQS, D + 2 * DK + DV), BF16...  43.4 us

profile of v4, /device:TPU:0, one launch (start us, length us, event | category | flops | bytes accessed | tf_op | source)
XLA Modules:
  0.0 44.8 jit_solution(1198398822895710724)
XLA Ops:
  0.6 43.4 %layer.1.packed = bf16[32,2304]{1,0:T(8,128)(2,1)S(1)} custom-call(bf16[32,2048]{1,0:T(8,128)(2,1)} %hidden_h.1, bf16[32,1024,128]{2,1,0:T(8,128)(2,1)} %keys_h.1, bf16[32,1024,128]{2,1,0:T(8,128)(2,1)} %values_h.1, s32[32]{0:T(128)} %lengths_h.1, f32[1,2048]{1,0:T(1,128)} %bitcast.5, bf16[2048,1024]{1,0:T(8,128)(2,1)} %wq_h.1, bf16[2048,128]{1,0:T(8,128)(2,1)} %wk_h.1, ...), custom_call_target="tpu_custom_call" | custom-call | tf_op jit(solution)/shard_map/layer/pallas_call | solution.py:384
  44.1 0.7 %finish.1 = (bf16[32,2048]{1,0:T(8,128)(2,1)}, bf16[32,128]{1,0:T(8,128)(2,1)}, bf16[32,128]{1,0:T(8,128)(2,1)}) custom-call(bf16[32,2304]{1,0:T(8,128)(2,1)S(1)} %layer.1.packed), custom_call_target="tpu_custom_call" | custom-call | tf_op jit(solution)/shard_map/finish/pallas_call | solution.py:395

commit v5 on v4

--- a/solution.py
+++ b/solution.py
@@ -139,15 +139,10 @@
     low = dot(low, spread)
     slot = iota((CHIPS * ROWS, lanes), 0)
     pick = jnp.zeros((CHIPS * ROWS, lanes), F32)
-    comb_high = jnp.zeros((CHIPS * ROWS, lanes), F32)
-    comb_low = jnp.zeros((CHIPS * ROWS, lanes), F32)
     for k in range(TOP_K):
         hit = slot == target[k : k + 1, :]
         pick = jnp.where(hit, 1.0, pick)
-        comb_high = jnp.where(hit, high[k : k + 1, :], comb_high)
-        comb_low = jnp.where(hit, low[k : k + 1, :], comb_low)
     picked[...] = pick.astype(BF16)
-    wcomb[...] = jnp.transpose(jnp.concatenate([comb_high, comb_low], axis=1)).astype(BF16)
 
     fetch_keys(0)
     small[2].wait()
@@ -255,8 +250,8 @@
     fetch_own()
     fresh_a = soften(0, highest_a, own_a)
     await_values(0)
+    fresh_b = soften(1, highest_b, own_b)
     gather(0, fresh_a)
-    fresh_b = soften(1, highest_b, own_b)
     await_values(1)
     gather(1, fresh_b)
     pl.semaphore_wait(barrier, CHIPS)
@@ -281,6 +276,13 @@
     for i, ref in enumerate((wg, wu, wd)):
         share(ref, i).start()
     recvbuf[0] = sendbuf[0]
+    comb_high = jnp.zeros((CHIPS * ROWS, lanes), F32)
+    comb_low = jnp.zeros((CHIPS * ROWS, lanes), F32)
+    for k in range(TOP_K):
+        hit = slot == target[k : k + 1, :]
+        comb_high = jnp.where(hit, high[k : k + 1, :], comb_high)
+        comb_low = jnp.where(hit, low[k : k + 1, :], comb_low)
+    wcomb[...] = jnp.transpose(jnp.concatenate([comb_high, comb_low], axis=1)).astype(BF16)
 
     size = PER * ROWS
     line = iota((size, size), 0)

time: 44.9 us -> 44.9 us (level)
  no operation moved by 1% of the time
where the time goes in v5:
time: 44.9 us; the launch traced here: 44.7 us
  Pallas kernels  44.1 us (98%)
  between operations  0.65 us (1%)
    pallas_call x1, Pallas kernels, per_device(): pl.pallas_call(kernel, out_shape=pltpu.VMEM((SEQS, D + 2 * DK + DV), BF16...  43.4 us

profile of v5, /device:TPU:0, one launch (start us, length us, event | category | flops | bytes accessed | tf_op | source)
XLA Modules:
  0.0 44.7 jit_solution(15332418631494976154)
XLA Ops:
  0.6 43.4 %layer.1.packed = bf16[32,2304]{1,0:T(8,128)(2,1)S(1)} custom-call(bf16[32,2048]{1,0:T(8,128)(2,1)} %hidden_h.1, bf16[32,1024,128]{2,1,0:T(8,128)(2,1)} %keys_h.1, bf16[32,1024,128]{2,1,0:T(8,128)(2,1)} %values_h.1, s32[32]{0:T(128)} %lengths_h.1, f32[1,2048]{1,0:T(1,128)} %bitcast.5, bf16[2048,1024]{1,0:T(8,128)(2,1)} %wq_h.1, bf16[2048,128]{1,0:T(8,128)(2,1)} %wk_h.1, ...), custom_call_target="tpu_custom_call" | custom-call | tf_op jit(solution)/shard_map/layer/pallas_call | solution.py:386
  44.1 0.7 %finish.1 = (bf16[32,2048]{1,0:T(8,128)(2,1)}, bf16[32,128]{1,0:T(8,128)(2,1)}, bf16[32,128]{1,0:T(8,128)(2,1)}) custom-call(bf16[32,2304]{1,0:T(8,128)(2,1)S(1)} %layer.1.packed), custom_call_target="tpu_custom_call" | custom-call | tf_op jit(solution)/shard_map/finish/pallas_call | solution.py:397
